TPU v7x, 32 devices: a whole 2x2x4 slice. The times are simulated.
32 devices in a mesh: fs: 8 (over z, y), tp: 4 (over x, core).
Axes of the slice: x: 2, y: 2, z: 4, core: 2. Of those that a mesh axis runs over, the one named last changes fastest.
Arguments:
- later_input: bfloat16 [4096, 2048], P(('fs', 'tp')), may hold values from -6 to 6
- earlier_input: bfloat16 [4096, 2048], P('fs'), may hold values from -6 to 6
- earlier_hidden: bfloat16 [4096, 4096], P('fs', 'tp'), may hold values from -6 to 6
- cotangent: bfloat16 [4096, 2048], P('fs'), may hold values from -6 to 6
- up_weight: bfloat16 [2048, 4096], P('fs', 'tp'), may hold values from -0.125 to 0.125
- down_weight: bfloat16 [4096, 2048], P(('tp', 'fs')), may hold values from -0.09375 to 0.09375
- up_sum: float32 [2048, 4096], P('fs', 'tp'), may hold values from -4 to 4
- down_sum: float32 [4096, 2048], P(('tp', 'fs')), may hold values from -4 to 4
Outputs:
- later_output: bfloat16 [4096, 2048], P(('fs', 'tp'))
- later_hidden: bfloat16 [4096, 4096], P('fs', 'tp')
- earlier_grad: bfloat16 [4096, 2048], P(('fs', 'tp'))
- up_sum_next: float32 [2048, 4096], P('fs', 'tp')
- down_sum_next: float32 [4096, 2048], P(('tp', 'fs'))
All inputs are finite; a program needn't handle non-finite values.
Results may differ from a plain program's by a relative error of at most 0.0095.
Values may be sent and summed in bfloat16 or wider, within the bound.
A program may use at most 128 MiB of HBM per device.

v0:
```python
import jax
import jax.numpy as jnp
from jax import lax
from jax.sharding import PartitionSpec as P


def contract_last(left_rows, right_rows):
    return lax.dot_general(
        left_rows, right_rows, (((1,), (1,)), ((), ())), preferred_element_type=jnp.float32
    )


def contract_first(left_rows, right_rows):
    return lax.dot_general(
        left_rows, right_rows, (((0,), (0,)), ((), ())), preferred_element_type=jnp.float32
    )


def shards(
    later_input, earlier_input, earlier_hidden, cotangent, up_weight, down_weight, up_sum, down_sum
):
    gathered = lax.all_gather(later_input, "tp", axis=0, tiled=True)
    groups = lax.axis_size("fs")
    grad_scale = float(earlier_input.shape[0] * groups) ** (-0.5)
    lifted = jnp.maximum(earlier_hidden.astype(jnp.float32), 0.0)
    activation = (lifted * lifted).astype(jnp.bfloat16)
    up_front, down_front = (
        lax.all_gather(up_weight, "fs", axis=0, tiled=True),
        lax.all_gather(down_weight, "fs", axis=0, tiled=True),
    )
    later_hidden = jnp.dot(gathered, up_front, preferred_element_type=jnp.float32).astype(
        jnp.bfloat16
    )
    lifted_later = jnp.maximum(later_hidden.astype(jnp.float32), 0.0)
    act_later = (lifted_later * lifted_later).astype(jnp.bfloat16)
    rows_here = act_later
    later_output = lax.psum_scatter(
        jnp.dot(rows_here, down_front, preferred_element_type=jnp.float32).astype(jnp.bfloat16),
        "tp",
        scatter_dimension=0,
        tiled=True,
    )
    up_back, down_back = (up_front, down_front)
    act_slope = contract_last(cotangent, down_back)
    pre_grad = (2.0 * act_slope * lifted).astype(jnp.bfloat16)
    rows_here = pre_grad
    earlier_grad = lax.psum_scatter(
        contract_last(rows_here, up_back).astype(jnp.bfloat16),
        "tp",
        scatter_dimension=0,
        tiled=True,
    )
    columns = earlier_input
    up_total = lax.psum_scatter(
        contract_first(columns, pre_grad), "fs", scatter_dimension=0, tiled=True
    )
    earlier_grad, up_total = (earlier_grad, up_total)
    columns = activation
    down_total = lax.psum_scatter(
        contract_first(columns, cotangent), "fs", scatter_dimension=0, tiled=True
    )
    return (
        later_output,
        later_hidden,
        earlier_grad,
        up_sum + grad_scale * up_total,
        down_sum + grad_scale * down_total,
    )


def solution(mesh):
    in_specs = (
        P(("fs", "tp"), None),
        P("fs", None),
        P("fs", "tp"),
        P("fs", None),
        P("fs", "tp"),
        P(("tp", "fs"), None),
        P("fs", "tp"),
        P(("tp", "fs"), None),
    )
    out_specs = (
        P(("fs", "tp"), None),
        P("fs", "tp"),
        P(("fs", "tp"), None),
        P("fs", "tp"),
        P(("tp", "fs"), None),
    )
    return jax.shard_map(shards, mesh=mesh, in_specs=in_specs, out_specs=out_specs, check_vma=False)
```

profile of v0, /device:TPU:0, one launch (start us, length us, event | category | flops | bytes accessed | tf_op | source)
XLA Modules:
  0.0 557.7 jit_solution(5843369301261905202)
XLA Ops:
  7.2 0.0 copy-start
  7.2 0.0 all-gather.8.cloned.1.call-start
  7.2 0.7 all-gather.8.cloned.1.call-update
  7.9 0.0 all-gather.6.cloned.1.call-start
  8.0 0.7 all-gather.6.cloned.1.call-update
  8.7 0.0 all-gather.4.cloned.1.call-start
  8.7 0.7 all-gather.4.cloned.1.call-update
  9.4 0.0 reduce-scatter.11.cloned.1.call-start
  9.4 0.0 copy-done
  9.5 6.9 %fusion = f32[1024,2048]{1,0:T(8,128)} fusion(bf16[512,2048]{1,0:T(8,128)(2,1)S(1)} %copy-done, bf16[512,1024]{1,0:T(8,128)(2,1)} %param.10), kind=kOutput, calls=%fused_computation.8 | convolution fusion | flops 2149580800 | bytes 11534336 | tf_op jit(solution)/shard_map/dot_general | solution.py:14
  16.3 0.0 copy-start.3
  16.3 0.0 reduce-scatter.11.cloned.1.call-update
  16.3 0.0 reduce-scatter.9.cloned.1.call-start
  16.4 69.3 %all-gather.8.cloned.1.call-done = bf16[1024,2048]{1,0:T(8,128)(2,1)} async-done(((bf16[128,2048]{1,0:T(8,128)(2,1)}), bf16[1024,2048]{1,0:T(8,128)(2,1)}) %all-gather.8.cloned.1.call-update) | async-done | bytes 4194320 | tf_op jit(solution)/shard_map/all_gather | solution.py:29
  85.7 0.0 copy-done.3
  85.7 0.0 copy-start.2
  85.7 4.7 multiply_convert_fusion.1
  90.4 0.0 copy-start.5
  90.4 1.0 copy-done.5
  91.4 0.0 copy-done.2
  91.4 5.6 %convolution_bitcast_fusion = f32[2048,1024]{0,1:T(8,128)} fusion(bf16[512,1024]{1,0:T(8,128)(2,1)S(1)} %multiply_convert_fusion.1, bf16[512,2048]{1,0:T(8,128)(2,1)S(1)} %copy-done.2), kind=kOutput, calls=%fused_computation | convolution fusion | flops 2147483648 | bytes 11534336 | tf_op jit(solution)/shard_map/dot_general | solution.py:14
  97.0 0.0 copy-start.6
  97.0 0.0 reduce-scatter.9.cloned.1.call-update
  97.0 0.0 reduce-scatter.7.cloned.1.call-start
  97.1 62.1 %all-gather.6.cloned.1.call-done = bf16[2048,1024]{1,0:T(8,128)(2,1)} async-done(((bf16[256,1024]{1,0:T(8,128)(2,1)}), bf16[2048,1024]{1,0:T(8,128)(2,1)}) %all-gather.6.cloned.1.call-update) | async-done | bytes 4194320 | tf_op jit(solution)/shard_map/all_gather | solution.py:28
  159.1 0.0 copy-done.6
  159.1 5.9 %convolution_convert_fusion = bf16[512,2048]{1,0:T(8,128)(2,1)} fusion(bf16[512,1024]{1,0:T(8,128)(2,1)S(1)} %copy-done.6, bf16[2048,1024]{1,0:T(8,128)(2,1)} %all-gather.6.cloned.1.call-done), kind=kOutput, calls=%fused_computation.1 | convolution fusion | flops 2148532224 | bytes 7340032 | tf_op jit(solution)/shard_map/dot_general | solution.py:8
  165.1 0.0 reduce-scatter.7.cloned.1.call-update
  165.1 0.2 reduce-scatter.5.cloned.1.call-start
  165.3 16.5 %all-gather.4.cloned.1.call-done = bf16[512,2048]{1,0:T(8,128)(2,1)} async-done(((bf16[128,2048]{1,0:T(8,128)(2,1)}), bf16[512,2048]{1,0:T(8,128)(2,1)}) %all-gather.4.cloned.1.call-update) | async-done | bytes 2097168 | tf_op jit(solution)/shard_map/all_gather | solution.py:22
  181.8 0.0 copy-start.1
  181.8 5.3 convolution_convert_fusion.2
  187.1 0.0 copy-start.4
  187.2 1.0 copy-done.4
  188.1 0.0 copy-done.1
  188.1 3.7 convolution_convert_fusion.1
  191.8 0.0 reduce-scatter.5.cloned.1.call-update
  191.8 1.9 copy.13
  193.7 139.1 %reduce-scatter.11.cloned.1.call-done = f32[128,2048]{1,0:T(8,128)} async-done(((f32[1024,2048]{1,0:T(8,128)}), f32[128,2048]{1,0:T(8,128)}) %reduce-scatter.11.cloned.1.call-update) | async-done | bytes 1048592 | tf_op jit(solution)/shard_map/reduce_scatter | solution.py:59
  332.8 2.6 multiply_add_fusion
  335.5 147.8 %reduce-scatter.9.cloned.1.call-done = f32[256,1024]{0,1:T(8,128)} async-done(((f32[2048,1024]{0,1:T(8,128)}), f32[256,1024]{0,1:T(8,128)}) %reduce-scatter.9.cloned.1.call-update) | async-done | bytes 1048592 | tf_op jit(solution)/shard_map/reduce_scatter | solution.py:54
  483.3 2.3 multiply_add_fusion.1
  485.6 2.5 copy.14
  488.2 28.4 %reduce-scatter.7.cloned.1.call-done = bf16[128,2048]{1,0:T(8,128)(2,1)} async-done(((bf16[512,2048]{1,0:T(8,128)(2,1)}), bf16[128,2048]{1,0:T(8,128)(2,1)}) %reduce-scatter.7.cloned.1.call-update) | async-done | bytes 524304 | tf_op jit(solution)/shard_map/reduce_scatter | solution.py:47
  516.6 34.3 %reduce-scatter.5.cloned.1.call-done = bf16[128,2048]{1,0:T(8,128)(2,1)} async-done(((bf16[512,2048]{1,0:T(8,128)(2,1)}), bf16[128,2048]{1,0:T(8,128)(2,1)}) %reduce-scatter.5.cloned.1.call-update) | async-done | bytes 524304 | tf_op jit(solution)/shard_map/reduce_scatter | solution.py:37
Async XLA Ops:
  7.2 2.3 copy-start
  7.2 78.5 %all-gather.8.cloned.1.call-start = ((), (), s32[]{:S(2)}) async-start(), calls=%async_computation.6 | async-start | bytes 4718592 | tf_op jit(solution)/shard_map/all_gather | solution.py:29
  7.9 151.2 %all-gather.6.cloned.1.call-start = ((), (), s32[]{:S(2)}) async-start(), calls=%async_computation.5 | async-start | bytes 4718592 | tf_op jit(solution)/shard_map/all_gather | solution.py:28
  8.7 173.2 %all-gather.4.cloned.1.call-start = ((), (), s32[]{:S(2)}) async-start(), calls=%async_computation.4 | async-start | bytes 2621440 | tf_op jit(solution)/shard_map/all_gather | solution.py:22
  9.4 323.4 %reduce-scatter.11.cloned.1.call-start = ((), (), s32[]{:S(2)}) async-start(), calls=%async_computation.10 | async-start | bytes 9437184 | tf_op jit(solution)/shard_map/reduce_scatter | solution.py:59
  16.3 69.3 %copy-start.3 = (bf16[512,1024]{1,0:T(8,128)(2,1)S(1)}, bf16[512,1024]{1,0:T(8,128)(2,1)}, u32[]{:S(2)}) copy-start(bf16[512,1024]{1,0:T(8,128)(2,1)} %param.10) | copy-start | bytes 3145732
  16.3 467.0 %reduce-scatter.9.cloned.1.call-start = ((), (), s32[]{:S(2)}) async-start(), calls=%async_computation.9 | async-start | bytes 9437184 | tf_op jit(solution)/shard_map/reduce_scatter | solution.py:54
  85.7 5.7 %copy-start.2 = (bf16[512,2048]{1,0:T(8,128)(2,1)S(1)}, bf16[512,2048]{1,0:T(8,128)(2,1)}, u32[]{:S(2)}) copy-start(bf16[512,2048]{1,0:T(8,128)(2,1)} %param.9) | copy-start | bytes 6291460
  90.4 1.0 copy-start.5
  97.0 62.2 %copy-start.6 = (bf16[512,1024]{1,0:T(8,128)(2,1)S(1)}, bf16[512,1024]{1,0:T(8,128)(2,1)}, u32[]{:S(2)}) copy-start(bf16[512,1024]{1,0:T(8,128)(2,1)} %copy-done.5) | copy-start | bytes 3145732
  97.0 419.6 %reduce-scatter.7.cloned.1.call-start = ((), (), s32[]{:S(2)}) async-start(), calls=%async_computation.8 | async-start | bytes 2621440 | tf_op jit(solution)/shard_map/reduce_scatter | solution.py:47
  165.1 385.8 %reduce-scatter.5.cloned.1.call-start = ((), (), s32[]{:S(2)}) async-start(), calls=%async_computation.7 | async-start | bytes 2621440 | tf_op jit(solution)/shard_map/reduce_scatter | solution.py:37
  181.8 6.3 %copy-start.1 = (bf16[1024,2048]{1,0:T(8,128)(2,1)S(1)}, bf16[1024,2048]{1,0:T(8,128)(2,1)}, u32[]{:S(2)}) copy-start(bf16[1024,2048]{1,0:T(8,128)(2,1)} %all-gather.8.cloned.1.call-done) | copy-start | bytes 12582916
  187.1 1.0 copy-start.4
Sparse Core Ops, SparseCore 0:
  10.1 75.5 all-gather.7
  87.8 71.3 all-gather.5
  160.7 21.0 all-gather.3
  185.3 147.4 reduce-scatter.10
  336.3 146.9 reduce-scatter.8
  486.3 30.2 reduce-scatter.6
  519.7 31.1 reduce-scatter.4
where the time goes:
time: 558 us
  waiting for transfers between devices  500 us (90%)
  matrix products  32.1 us (6%)
  between operations  14.2 us (3%)
  local copies, waits for them, and re-layouts  6.36 us (1%)
    reduce_scatter x1, waiting for transfers between devices, shards(): lax.psum_scatter(contract_first(columns, pre_grad), 'fs', scatter_dimensi...  148 us
    reduce_scatter x1, waiting for transfers between devices, shards(): lax.psum_scatter(contract_first(columns, cotangent), 'fs', scatter_dimens...  139 us
    all_gather x1, waiting for transfers between devices, shards(): lax.all_gather(down_weight, 'fs', axis=0, tiled=True)  69.3 us
    all_gather x1, waiting for transfers between devices, shards(): lax.all_gather(up_weight, 'fs', axis=0, tiled=True)  62.1 us
    reduce_scatter x1, waiting for transfers between devices, shards(): lax.psum_scatter(jnp.dot(rows_here, down_front, preferred_element_type=jn...  34.3 us
    reduce_scatter x1, waiting for transfers between devices, shards(): lax.psum_scatter(contract_last(rows_here, up_back).astype(jnp.bfloat16),...  28.4 us
    all_gather x1, waiting for transfers between devices, shards(): gathered = lax.all_gather(later_input, 'tp', axis=0, tiled=True)  16.5 us
    dot_general x2, matrix products, contract_first(): lax.dot_general(left_rows, right_rows, (((0,), (0,)), ((), ())), preferre...  12.5 us
  transfers between devices with their start and end apart: 7, of which 7 were waited for; matrix products, arithmetic and copies ran while one was open for 7% of the time, Pallas kernels for 0%

commit v1 on v0

--- a/solution.py
+++ b/solution.py
@@ -2,6 +2,27 @@
 import jax.numpy as jnp
 from jax import lax
 from jax.sharding import PartitionSpec as P
+
+
+def _search_sources_all(inp, link_axis, in_dim):
+    chips = lax.axis_size(link_axis)
+    e_next = map(lambda at: (at, (at + 1) % chips), range(chips))
+    bank = list(e_next)
+    local_next = range(chips)
+    rows = list(map(lambda at: (at, (at - 1) % chips), local_next))
+    w1, parts_out = ([inp], [inp])
+    for _ in range(chips // 2):
+        right_arr = lax.ppermute(w1[-1], axis_name=link_axis, perm=bank)
+        w1.append(right_arr)
+    c = 0
+    while c < (chips - 1) // 2:
+        x_new = lax.ppermute(parts_out[-1], perm=rows, axis_name=link_axis)
+        parts_out.append(x_new)
+        c += 1
+    passed = jnp.concatenate([*w1[::-1], *parts_out[1:]], in_dim)
+    finding = lax.axis_index(link_axis)
+    f_next = jnp.roll(passed, (finding - chips // 2) * inp.shape[in_dim], in_dim)
+    return f_next
 
 
 def contract_last(left_rows, right_rows):
@@ -25,7 +46,7 @@
     lifted = jnp.maximum(earlier_hidden.astype(jnp.float32), 0.0)
     activation = (lifted * lifted).astype(jnp.bfloat16)
     up_front, down_front = (
-        lax.all_gather(up_weight, "fs", axis=0, tiled=True),
+        _search_sources_all(up_weight, "fs", 0),
         lax.all_gather(down_weight, "fs", axis=0, tiled=True),
     )
     later_hidden = jnp.dot(gathered, up_front, preferred_element_type=jnp.float32).astype(

time: 558 us -> 520 us (0.932)
  waiting for transfers between devices: 500 us -> 427 us
  starting transfers between devices: 0.46 us -> 21.4 us
  local copies, waits for them, and re-layouts: 6.36 us -> 23.1 us
    ppermute x0 -> x7, waiting for transfers between devices: none -> 82.5 us  [the longest x4 74.9 us: _search_sources_all(): right_arr = lax.ppermute(w1[-1], axis_name=link_axis, perm=bank)]
    reduce_scatter x1, waiting for transfers between devices: 139 us -> 63.1 us  [shards(): lax.psum_scatter(contract_first(columns, cotangent), 'fs', scatter_dimens...]
    all_gather x1 -> x0, waiting for transfers between devices: 62.1 us -> none  [shards(): lax.all_gather(up_weight, 'fs', axis=0, tiled=True)]
    ppermute x0 -> x7, starting transfers between devices: none -> 21 us  [the longest x3 17.9 us: _search_sources_all(): x_new = lax.ppermute(parts_out[-1], perm=rows, axis_name=link_axis)]
    unnamed x16 -> x39, local copies, waits for them, and re-layouts: 6.36 us -> 23 us
    all_gather x1, waiting for transfers between devices: 16.5 us -> 0.02 us  [shards(): gathered = lax.all_gather(later_input, 'tp', axis=0, tiled=True)]
  transfers between devices with their start and end apart: 7 -> 13, of which waited for: 7 -> 11; matrix products, arithmetic and copies ran while one was open for 7% -> 10% of each run, Pallas kernels for 0% -> 0%
where the time goes in v1:
time: 520 us
  waiting for transfers between devices  427 us (82%)
  matrix products  28.7 us (6%)
  local copies, waits for them, and re-layouts  23.1 us (4%)
  starting transfers between devices  21.4 us (4%)
  between operations  14.3 us (3%)
    reduce_scatter x1, waiting for transfers between devices, shards(): lax.psum_scatter(contract_first(columns, pre_grad), 'fs', scatter_dimensi...  148 us
    ppermute x4, waiting for transfers between devices, _search_sources_all(): right_arr = lax.ppermute(w1[-1], axis_name=link_axis, perm=bank)  74.9 us
    all_gather x1, waiting for transfers between devices, shards(): lax.all_gather(down_weight, 'fs', axis=0, tiled=True)  69.8 us
    reduce_scatter x1, waiting for transfers between devices, shards(): lax.psum_scatter(contract_first(columns, cotangent), 'fs', scatter_dimens...  63.1 us
    reduce_scatter x1, waiting for transfers between devices, shards(): lax.psum_scatter(jnp.dot(rows_here, down_front, preferred_element_type=jn...  34.2 us
    reduce_scatter x1, waiting for transfers between devices, shards(): lax.psum_scatter(contract_last(rows_here, up_back).astype(jnp.bfloat16),...  28.4 us
    unnamed x39, local copies, waits for them, and re-layouts  23 us
    ppermute x3, starting transfers between devices, _search_sources_all(): x_new = lax.ppermute(parts_out[-1], perm=rows, axis_name=link_axis)  17.9 us
  transfers between devices with their start and end apart: 13, of which 11 were waited for; matrix products, arithmetic and copies ran while one was open for 10% of the time, Pallas kernels for 0%

profile of v1, /device:TPU:0, one launch (start us, length us, event | category | flops | bytes accessed | tf_op | source)
XLA Modules:
  0.0 519.6 jit_solution(17361724582019339988)
XLA Ops:
  7.2 0.0 copy-start
  7.2 0.0 all-gather.5.cloned.1.call-start
  7.2 0.7 all-gather.5.cloned.1.call-update
  7.9 0.0 all-gather.3.cloned.1.call-start
  8.0 0.7 all-gather.3.cloned.1.call-update
  8.7 0.0 reduce-scatter.11.cloned.1.call-start
  8.7 1.5 copy.14
  10.2 0.0 copy-done
  10.2 5.6 %fusion.13 = f32[1024,2048]{1,0:T(8,128)} fusion(bf16[512,2048]{1,0:T(8,128)(2,1)S(1)} %copy-done, bf16[512,1024]{0,1:T(8,128)(2,1)S(1)} %copy.14), kind=kOutput, calls=%fused_computation.13 | convolution fusion | flops 2149580800 | bytes 11534336 | tf_op jit(solution)/shard_map/dot_general | solution.py:35
  15.8 0.0 reduce-scatter.11.cloned.1.call-update
  15.8 0.0 reduce-scatter.9.cloned.1.call-start
  15.9 69.8 %all-gather.5.cloned.1.call-done = bf16[1024,2048]{1,0:T(8,128)(2,1)} async-done(((bf16[128,2048]{1,0:T(8,128)(2,1)}), bf16[1024,2048]{1,0:T(8,128)(2,1)}) %all-gather.5.cloned.1.call-update) | async-done | bytes 4194320 | tf_op jit(solution)/shard_map/all_gather | solution.py:50
  85.7 4.7 multiply_convert_fusion.1
  90.4 0.0 copy-start.8
  90.4 1.0 copy-done.8
  91.4 0.0 copy-done.7
  91.4 5.6 %convolution_bitcast_fusion = f32[2048,1024]{0,1:T(8,128)} fusion(bf16[512,1024]{0,1:T(8,128)(2,1)S(1)} %multiply_convert_fusion.1, bf16[512,2048]{1,0:T(8,128)(2,1)S(1)} %copy-done.7), kind=kOutput, calls=%fused_computation | convolution fusion | flops 2147483648 | bytes 11534336 | tf_op jit(solution)/shard_map/dot_general | solution.py:35
  97.0 0.0 reduce-scatter.9.cloned.1.call-update
  97.0 0.0 reduce-scatter.7.cloned.1.call-start
  97.0 0.0 copy-done.1
  97.0 0.6 collective-permute-start
  97.6 14.6 %collective-permute-done = bf16[256,1024]{1,0:T(8,128)(2,1)S(1)} collective-permute-done((bf16[256,1024]{1,0:T(8,128)(2,1)S(1)}, bf16[256,1024]{1,0:T(8,128)(2,1)S(1)}, u32[]{:S(2)}, u32[]{:S(2)}) %collective-permute-start) | collective-permute-done | bytes 524320 | tf_op jit(solution)/shard_map/ppermute | solution.py:15
  112.2 0.0 collective-permute-start.1
  112.2 4.7 collective-permute-start.4
  117.0 27.1 %collective-permute-done.1 = bf16[256,1024]{1,0:T(8,128)(2,1)S(1)} collective-permute-done((bf16[256,1024]{1,0:T(8,128)(2,1)S(1)}, bf16[256,1024]{1,0:T(8,128)(2,1)S(1)}, u32[]{:S(2)}, u32[]{:S(2)}) %collective-permute-start.1) | collective-permute-done | bytes 524320 | tf_op jit(solution)/shard_map/ppermute | solution.py:15
  144.1 2.5 collective-permute-start.2
  146.6 0.0 collective-permute-done.4
  146.6 0.0 copy-done.2
  146.6 8.0 %collective-permute-start.5 = (bf16[256,1024]{1,0:T(8,128)(2,1)}, bf16[256,1024]{1,0:T(8,128)(2,1)}, u32[]{:S(2)}, u32[]{:S(2)}) collective-permute-start(bf16[256,1024]{1,0:T(8,128)(2,1)} %collective-permute-done.4), channel_id=1, source_target_pairs={{0,28},{4,0},{8,4},{12,8},{16,12},{20,16},{24,20},{28,24},{1,29},{... | collective-permute-start | bytes 1572872 | tf_op jit(solution)/shard_map/ppermute | solution.py:19
  154.6 16.7 %collective-permute-done.2 = bf16[256,1024]{1,0:T(8,128)(2,1)} collective-permute-done((bf16[256,1024]{1,0:T(8,128)(2,1)S(1)}, bf16[256,1024]{1,0:T(8,128)(2,1)}, u32[]{:S(2)}, u32[]{:S(2)}) %collective-permute-start.2) | collective-permute-done | bytes 524320 | tf_op jit(solution)/shard_map/ppermute | solution.py:15
  171.3 0.0 collective-permute-start.3
  171.3 6.5 %collective-permute-done.5 = bf16[256,1024]{1,0:T(8,128)(2,1)} collective-permute-done((bf16[256,1024]{1,0:T(8,128)(2,1)}, bf16[256,1024]{1,0:T(8,128)(2,1)}, u32[]{:S(2)}, u32[]{:S(2)}) %collective-permute-start.5) | collective-permute-done | bytes 524320 | tf_op jit(solution)/shard_map/ppermute | solution.py:19
  177.8 5.2 collective-permute-start.6
  183.0 16.4 %collective-permute-done.3 = bf16[256,1024]{1,0:T(8,128)(2,1)} collective-permute-done((bf16[256,1024]{1,0:T(8,128)(2,1)}, bf16[256,1024]{1,0:T(8,128)(2,1)}, u32[]{:S(2)}, u32[]{:S(2)}) %collective-permute-start.3) | collective-permute-done | bytes 524320 | tf_op jit(solution)/shard_map/ppermute | solution.py:15
  199.4 1.1 constant_dynamic-update-slice_fusion.15
  200.5 1.1 constant_dynamic-update-slice_fusion.14
  201.6 1.1 constant_dynamic-update-slice_fusion.13
  202.7 1.1 constant_dynamic-update-slice_fusion.10
  203.8 1.1 constant_dynamic-update-slice_fusion.9
  204.9 1.1 collective-permute-done.6
  206.1 1.1 constant_dynamic-update-slice_fusion.7
  207.2 1.1 constant_dynamic-update-slice_fusion.6
  208.4 1.1 constant_dynamic-update-slice_fusion.2
  209.5 1.1 constant_dynamic-update-slice_fusion.1
  210.6 3.2 copy-done.5
  213.9 0.0 copy-done.9
  213.9 3.7 fusion.4
  217.6 0.0 reduce-scatter.7.cloned.1.call-update
  217.6 0.2 reduce-scatter.5.cloned.1.call-start
  217.8 0.0 all-gather.3.cloned.1.call-done
  217.8 5.4 %fusion.10 = bf16[512,1024]{0,1:T(8,128)(2,1)S(1)} fusion(bf16[512,2048]{1,0:T(8,128)(2,1)} %all-gather.3.cloned.1.call-done, bf16[4096,1024]{1,0:T(8,128)(2,1)} %copy-done.5, s32[]{:T(128)S(6)} %select_n.14), kind=kOutput, calls=%fused_computation.12 | convolution fusion | flops 2148007936 | bytes 7340036 | tf_op jit(solution)/shard_map/dot_general | solution.py:52
  223.2 0.0 copy-start.4
  223.3 1.0 copy-done.4
  224.2 3.7 convolution_convert_fusion
  227.9 0.0 reduce-scatter.5.cloned.1.call-update
  228.0 1.6 copy.15
  229.5 2.3 copy.16
  231.8 63.1 %reduce-scatter.11.cloned.1.call-done = f32[128,2048]{1,0:T(8,128)} async-done(((f32[1024,2048]{1,0:T(8,128)}), f32[128,2048]{1,0:T(8,128)}) %reduce-scatter.11.cloned.1.call-update) | async-done | bytes 1048592 | tf_op jit(solution)/shard_map/reduce_scatter | solution.py:80
  294.9 2.6 multiply_add_fusion
  297.5 147.8 %reduce-scatter.9.cloned.1.call-done = f32[256,1024]{0,1:T(8,128)} async-done(((f32[2048,1024]{0,1:T(8,128)}), f32[256,1024]{0,1:T(8,128)}) %reduce-scatter.9.cloned.1.call-update) | async-done | bytes 1048592 | tf_op jit(solution)/shard_map/reduce_scatter | solution.py:75
  445.3 2.3 multiply_add_fusion.1
  447.7 2.5 copy.17
  450.2 28.4 %reduce-scatter.7.cloned.1.call-done = bf16[128,2048]{1,0:T(8,128)(2,1)} async-done(((bf16[512,2048]{1,0:T(8,128)(2,1)}), bf16[128,2048]{1,0:T(8,128)(2,1)}) %reduce-scatter.7.cloned.1.call-update) | async-done | bytes 524304 | tf_op jit(solution)/shard_map/reduce_scatter | solution.py:68
  478.6 34.2 %reduce-scatter.5.cloned.1.call-done = bf16[128,2048]{1,0:T(8,128)(2,1)} async-done(((bf16[512,2048]{1,0:T(8,128)(2,1)}), bf16[128,2048]{1,0:T(8,128)(2,1)}) %reduce-scatter.5.cloned.1.call-update) | async-done | bytes 524304 | tf_op jit(solution)/shard_map/reduce_scatter | solution.py:58
  (16 shorter events, 0.3 us)
Async XLA Ops:
  7.2 3.1 copy-start
  7.2 78.5 %all-gather.5.cloned.1.call-start = ((), (), s32[]{:S(2)}) async-start(), calls=%async_computation.5 | async-start | bytes 4718592 | tf_op jit(solution)/shard_map/all_gather | solution.py:50
  7.9 209.9 %all-gather.3.cloned.1.call-start = ((), (), s32[]{:S(2)}) async-start(), calls=%async_computation.4 | async-start | bytes 2621440 | tf_op jit(solution)/shard_map/all_gather | solution.py:43
  8.7 286.2 %reduce-scatter.11.cloned.1.call-start = ((), (), s32[]{:S(2)}) async-start(), calls=%async_computation.9 | async-start | bytes 9437184 | tf_op jit(solution)/shard_map/reduce_scatter | solution.py:80
  15.8 429.5 %reduce-scatter.9.cloned.1.call-start = ((), (), s32[]{:S(2)}) async-start(), calls=%async_computation.8 | async-start | bytes 9437184 | tf_op jit(solution)/shard_map/reduce_scatter | solution.py:75
  85.7 5.7 %copy-start.7 = (bf16[512,2048]{1,0:T(8,128)(2,1)S(1)}, bf16[512,2048]{1,0:T(8,128)(2,1)}, u32[]{:S(2)}) copy-start(bf16[512,2048]{1,0:T(8,128)(2,1)} %param.9) | copy-start | bytes 6291460
  90.4 1.0 copy-start.8
  91.4 5.7 %copy-start.1 = (bf16[256,1024]{1,0:T(8,128)(2,1)S(1)}, bf16[256,1024]{1,0:T(8,128)(2,1)}, u32[]{:S(2)}) copy-start(bf16[256,1024]{1,0:T(8,128)(2,1)} %param.12) | copy-start | bytes 1572868
  97.0 381.6 %reduce-scatter.7.cloned.1.call-start = ((), (), s32[]{:S(2)}) async-start(), calls=%async_computation.7 | async-start | bytes 2621440 | tf_op jit(solution)/shard_map/reduce_scatter | solution.py:68
  97.0 15.2 %collective-permute-start = (bf16[256,1024]{1,0:T(8,128)(2,1)S(1)}, bf16[256,1024]{1,0:T(8,128)(2,1)S(1)}, u32[]{:S(2)}, u32[]{:S(2)}) collective-permute-start(bf16[256,1024]{1,0:T(8,128)(2,1)S(1)} %copy-done.1), channel_id=1, source_target_pairs={{0,4},{4,8},{8,12},{12,16},{16,20},{20,24},{24,28},{28,0},{1,5},{5... | collective-permute-start | bytes 1572872 | tf_op jit(solution)/shard_map/ppermute | solution.py:15
  112.2 31.9 %collective-permute-start.1 = (bf16[256,1024]{1,0:T(8,128)(2,1)S(1)}, bf16[256,1024]{1,0:T(8,128)(2,1)S(1)}, u32[]{:S(2)}, u32[]{:S(2)}) collective-permute-start(bf16[256,1024]{1,0:T(8,128)(2,1)S(1)} %collective-permute-done), channel_id=1, source_target_pairs={{0,4},{4,8},{8,12},{12,16},{16,20},{20,24},{24,28},{28,0},{1,5},{5... | collective-permute-start | bytes 1572872 | tf_op jit(solution)/shard_map/ppermute | solution.py:15
  112.2 34.3 %collective-permute-start.4 = (bf16[256,1024]{1,0:T(8,128)(2,1)S(1)}, bf16[256,1024]{1,0:T(8,128)(2,1)}, u32[]{:S(2)}, u32[]{:S(2)}) collective-permute-start(bf16[256,1024]{1,0:T(8,128)(2,1)S(1)} %copy-done.1), channel_id=1, source_target_pairs={{0,28},{4,0},{8,4},{12,8},{16,12},{20,16},{24,20},{28,24},{1,29},{... | collective-permute-start | bytes 1572872 | tf_op jit(solution)/shard_map/ppermute | solution.py:19
  144.1 2.5 copy-start.2
  144.1 27.2 %collective-permute-start.2 = (bf16[256,1024]{1,0:T(8,128)(2,1)S(1)}, bf16[256,1024]{1,0:T(8,128)(2,1)}, u32[]{:S(2)}, u32[]{:S(2)}) collective-permute-start(bf16[256,1024]{1,0:T(8,128)(2,1)S(1)} %collective-permute-done.1), channel_id=1, source_target_pairs={{0,4},{4,8},{8,12},{12,16},{16,20},{20,24},{24,28},{28,0},{1,5},{5... | collective-permute-start | bytes 1572872 | tf_op jit(solution)/shard_map/ppermute | solution.py:15
  146.6 31.2 %collective-permute-start.5 = (bf16[256,1024]{1,0:T(8,128)(2,1)}, bf16[256,1024]{1,0:T(8,128)(2,1)}, u32[]{:S(2)}, u32[]{:S(2)}) collective-permute-start(bf16[256,1024]{1,0:T(8,128)(2,1)} %collective-permute-done.4), channel_id=1, source_target_pairs={{0,28},{4,0},{8,4},{12,8},{16,12},{20,16},{24,20},{28,24},{1,29},{... | collective-permute-start | bytes 1572872 | tf_op jit(solution)/shard_map/ppermute | solution.py:19
  171.3 28.1 %collective-permute-start.3 = (bf16[256,1024]{1,0:T(8,128)(2,1)}, bf16[256,1024]{1,0:T(8,128)(2,1)}, u32[]{:S(2)}, u32[]{:S(2)}) collective-permute-start(bf16[256,1024]{1,0:T(8,128)(2,1)} %collective-permute-done.2), channel_id=1, source_target_pairs={{0,4},{4,8},{8,12},{12,16},{16,20},{20,24},{24,28},{28,0},{1,5},{5... | collective-permute-start | bytes 1572872 | tf_op jit(solution)/shard_map/ppermute | solution.py:15
  171.3 37.0 %copy-start.3 = (bf16[256,1024]{1,0:T(8,128)(2,1)S(1)}, bf16[256,1024]{1,0:T(8,128)(2,1)}, u32[]{:S(2)}) copy-start(bf16[256,1024]{1,0:T(8,128)(2,1)} %copy-done.2) | copy-start | bytes 1572868
  171.3 42.6 %copy-start.9 = (bf16[512,1024]{0,1:T(8,128)(2,1)S(1)}, bf16[512,1024]{0,1:T(8,128)(2,1)}, u32[]{:S(2)}) copy-start(bf16[512,1024]{0,1:T(8,128)(2,1)} %copy-done.8) | copy-start | bytes 3145732
  177.8 28.2 %collective-permute-start.6 = (bf16[256,1024]{1,0:T(8,128)(2,1)}, bf16[256,1024]{1,0:T(8,128)(2,1)S(1)}, u32[]{:S(2)}, u32[]{:S(2)}) collective-permute-start(bf16[256,1024]{1,0:T(8,128)(2,1)} %collective-permute-done.5), channel_id=1, source_target_pairs={{0,28},{4,0},{8,4},{12,8},{16,12},{20,16},{24,20},{28,24},{1,29},{... | collective-permute-start | bytes 1572872 | tf_op jit(solution)/shard_map/ppermute | solution.py:19
  210.6 3.3 copy-start.5
  217.6 295.2 %reduce-scatter.5.cloned.1.call-start = ((), (), s32[]{:S(2)}) async-start(), calls=%async_computation.6 | async-start | bytes 2621440 | tf_op jit(solution)/shard_map/reduce_scatter | solution.py:58
  217.8 6.4 %copy-start.6 = (bf16[1024,2048]{1,0:T(8,128)(2,1)S(1)}, bf16[1024,2048]{1,0:T(8,128)(2,1)}, u32[]{:S(2)}) copy-start(bf16[1024,2048]{1,0:T(8,128)(2,1)} %all-gather.5.cloned.1.call-done) | copy-start | bytes 12582916
  223.2 1.0 copy-start.4
Sparse Core Ops, SparseCore 0:
  10.1 75.5 all-gather.4
  87.2 21.0 all-gather.2
  112.0 182.8 reduce-scatter.10
  298.4 146.9 reduce-scatter.8
  448.3 30.2 reduce-scatter.6
  481.6 31.1 reduce-scatter.4
